TPU v7x, 32 devices: a whole 2x2x4 slice. The times are simulated.
32 devices in a mesh: fs: 8 (over z, y), tp: 4 (over x, core).
Axes of the slice: x: 2, y: 2, z: 4, core: 2. Of those that a mesh axis runs over, the one named last changes fastest.
Arguments:
- inputs: bfloat16 [4096, 2048], P(('fs', 'tp')), may hold values from -6 to 6
- w_gate: float32 [2048, 5632], P('fs', 'tp'), may hold values from -0.125 to 0.125
- w_value: float32 [2048, 5632], P('fs', 'tp'), may hold values from -0.125 to 0.125
- gate_scale: float32 [5632], P('tp'), may hold values from 0.5 to 2
- value_scale: float32 [5632], P('tp'), may hold values from 0.5 to 2
- conv_gate: float32 [3, 5632], P(None, 'tp'), may hold values from -3.5 to 3.5
- conv_value: float32 [3, 5632], P(None, 'tp'), may hold values from -3.5 to 3.5
- gate_pre: bfloat16 [4096, 5632], P('fs', 'tp'), may hold values from -6 to 6
- value_pre: bfloat16 [4096, 5632], P('fs', 'tp'), may hold values from -6 to 6
- grad_out: bfloat16 [4096, 5632], P('fs', 'tp'), may hold values from -6 to 6
Outputs:
- grad_inputs: bfloat16 [4096, 2048], P(('fs', 'tp'))
- grad_w_gate: float32 [2048, 5632], P('fs', 'tp')
- grad_w_value: float32 [2048, 5632], P('fs', 'tp')
- grad_gate_scale: float32 [5632], P('tp')
- grad_value_scale: float32 [5632], P('tp')
- grad_conv_gate: float32 [3, 5632], P(None, 'tp')
- grad_conv_value: float32 [3, 5632], P(None, 'tp')
All inputs are finite; a program needn't handle non-finite values.
Results may differ from a plain program's by a relative error of at most 0.015.
Values may be sent and summed in bfloat16 or wider, within the bound.
No kernel may reach another device: no remote copies, remote signals or barrier semaphores. Data moves between devices by JAX's collectives and lax.ppermute only.
A program may use at most 128 MiB of HBM per device.

v0:
```python
import jax
import jax.numpy as jnp
from jax import lax
from jax.sharding import PartitionSpec as P


def shift_down(field, steps):
    return jnp.pad(field, ((steps, 0), (0, 0)))[: field.shape[0]]


def shift_up(field, steps):
    return jnp.pad(field, ((0, steps), (0, 0)))[steps:]


def on_device(
    inputs,
    w_gate,
    w_value,
    gate_scale,
    value_scale,
    conv_gate,
    conv_value,
    gate_pre,
    value_pre,
    grad_out,
):
    gate_raw = gate_pre.astype(jnp.float32)
    value_raw = value_pre.astype(jnp.float32)
    gate_lin = gate_raw * gate_scale
    value_lin = value_raw * value_scale
    gate_conv = (
        conv_gate[2] * gate_lin
        + conv_gate[1] * shift_down(gate_lin, 1)
        + conv_gate[0] * shift_down(gate_lin, 2)
    )
    value_conv = (
        conv_value[2] * value_lin
        + conv_value[1] * shift_down(value_lin, 1)
        + conv_value[0] * shift_down(value_lin, 2)
    )
    sig = jax.nn.sigmoid(gate_conv)
    upstream = grad_out.astype(jnp.float32)
    d_gate_conv = upstream * value_conv * sig * (1.0 + gate_conv * (1.0 - sig))
    d_value_conv = upstream * gate_conv * sig
    taps_gate = jnp.stack(
        [
            jnp.sum(d_gate_conv * shift_down(gate_lin, 2), axis=0),
            jnp.sum(d_gate_conv * shift_down(gate_lin, 1), axis=0),
            jnp.sum(d_gate_conv * gate_lin, axis=0),
        ]
    )
    taps_value = jnp.stack(
        [
            jnp.sum(d_value_conv * shift_down(value_lin, 2), axis=0),
            jnp.sum(d_value_conv * shift_down(value_lin, 1), axis=0),
            jnp.sum(d_value_conv * value_lin, axis=0),
        ]
    )
    d_gate_lin = (
        conv_gate[2] * d_gate_conv
        + conv_gate[1] * shift_up(d_gate_conv, 1)
        + conv_gate[0] * shift_up(d_gate_conv, 2)
    )
    d_value_lin = (
        conv_value[2] * d_value_conv
        + conv_value[1] * shift_up(d_value_conv, 1)
        + conv_value[0] * shift_up(d_value_conv, 2)
    )
    scale_gate = jnp.sum(d_gate_lin * gate_raw, axis=0)
    scale_value = jnp.sum(d_value_lin * value_raw, axis=0)
    sums = lax.psum((scale_gate, scale_value, taps_gate, taps_value), "fs")
    gate_cot = d_gate_lin.astype(jnp.bfloat16)
    value_cot = d_value_lin.astype(jnp.bfloat16)
    gate_back = (d_gate_lin * gate_scale).astype(jnp.bfloat16)
    value_back = (d_value_lin * value_scale).astype(jnp.bfloat16)
    columns = gate_pre.shape[1]
    gathered = lax.all_gather(inputs, "tp", axis=0, tiled=True)
    stacked = jnp.stack([w_gate.astype(jnp.bfloat16), w_value.astype(jnp.bfloat16)])
    piece = lax.all_gather(stacked, "fs", axis=1, tiled=True)
    term = lax.dot_general(
        gate_back, piece[0], (((1,), (1,)), ((), ())), preferred_element_type=jnp.float32
    )
    terms = term + lax.dot_general(
        value_back, piece[1], (((1,), (1,)), ((), ())), preferred_element_type=jnp.float32
    )
    grad_inputs = lax.psum_scatter(
        terms.astype(jnp.bfloat16), "tp", scatter_dimension=0, tiled=True
    )
    both_cot = jnp.concatenate([gate_cot, value_cot], axis=1)
    summed = lax.psum_scatter(
        lax.dot_general(
            gathered, both_cot, (((0,), (0,)), ((), ())), preferred_element_type=jnp.float32
        ).astype(jnp.bfloat16),
        "fs",
        scatter_dimension=0,
        tiled=True,
    ).astype(jnp.float32)
    grad_w_gate = summed[:, :columns] * gate_scale
    grad_w_value = summed[:, columns:] * value_scale
    return (grad_inputs, grad_w_gate, grad_w_value, sums[0], sums[1], sums[2], sums[3])


def solution(mesh):
    placed = (
        P(("fs", "tp"), None),
        P("fs", "tp"),
        P("fs", "tp"),
        P("tp"),
        P("tp"),
        P(None, "tp"),
        P(None, "tp"),
        P("fs", "tp"),
        P("fs", "tp"),
        P("fs", "tp"),
    )
    return jax.shard_map(
        on_device,
        mesh=mesh,
        in_specs=placed,
        out_specs=(
            P(("fs", "tp"), None),
            P("fs", "tp"),
            P("fs", "tp"),
            P("tp"),
            P("tp"),
            P(None, "tp"),
            P(None, "tp"),
        ),
        check_vma=False,
    )
```

profile of v0, /device:TPU:0, one launch (start us, length us, event | category | flops | bytes accessed | tf_op | source)
XLA Modules:
  0.0 436.7 jit_solution(16981446529934875252)
XLA Ops:
  7.2 0.0 all-gather.5.cloned.1.call-start
  7.2 0.7 all-gather.5.cloned.1.call-update
  7.9 0.0 all-gather.3.cloned.1.call-start
  7.9 1.9 convert_bitcast_fusion.1
  9.9 0.0 copy-start.8
  9.9 0.0 copy-start.9
  9.9 0.0 copy-start.2
  9.9 0.0 copy-start.4
  9.9 0.0 copy-start.6
  10.0 0.0 copy-start.7
  10.0 1.2 pad_maximum_fusion
  11.2 0.0 all-gather.3.cloned.1.call-update
  11.2 0.0 reduce-scatter.5.cloned.1.call-start
  11.3 0.0 copy-done.8
  11.3 0.0 copy-done.9
  11.3 0.1 slice_reduce_fusion.4
  11.4 0.4 copy-done.2
  11.8 0.4 copy-done.4
  12.2 0.0 copy-done.6
  12.3 0.0 copy-done.7
  12.3 0.0 copy-start.1
  12.3 0.4 convert_multiply_fusion.1
  12.6 1.0 copy-done.1
  13.6 0.0 copy-start.3
  13.6 2.8 fusion.11
  16.4 0.0 copy-done.3
  16.5 2.3 multiply_reduce_fusion.5
  18.8 1.3 convert_element_type.63
  20.1 0.0 copy-start.5
  20.1 0.8 fusion.12
  20.9 0.6 copy-done.5
  21.5 2.3 multiply_reduce_fusion.2
  23.8 0.0 copy-start
  23.8 1.6 copy-done
  25.4 1.2 convert_element_type.64
  26.7 8.2 %all-gather.5.cloned.1.call-done = bf16[512,2048]{1,0:T(8,128)(2,1)} async-done(((bf16[128,2048]{1,0:T(8,128)(2,1)}), bf16[512,2048]{1,0:T(8,128)(2,1)}) %all-gather.5.cloned.1.call-update) | async-done | bytes 2097168 | tf_op jit(solution)/shard_map/all_gather | solution.py:77
  34.9 11.3 %convert_bitcast_fusion = bf16[2048,2816]{0,1:T(8,128)(2,1)} fusion(bf16[512,2048]{1,0:T(8,128)(2,1)} %all-gather.5.cloned.1.call-done, bf16[512,1408]{1,0:T(8,128)(2,1)} %convert_element_type.64, bf16[512,1408]{1,0:T(8,128)(2,1)} %convert_element_type.63), kind=kOutput, calls=%fused_computation | convolution fusion | flops 5917114368 | bytes 16515072 | tf_op jit(solution)/shard_map/dot_general | solution.py:91
  46.1 0.0 reduce-scatter.5.cloned.1.call-update
  46.2 0.2 reduce-scatter.3.cloned.1.call-start
  46.4 154.6 %all-gather.3.cloned.1.call-done = bf16[2,2048,1408]{2,1,0:T(8,128)(2,1)} async-done(((bf16[2,256,1408]{2,1,0:T(8,128)(2,1)}), bf16[2,2048,1408]{2,1,0:T(8,128)(2,1)}) %all-gather.3.cloned.1.call-update) | async-done | bytes 11534352 | tf_op jit(solution)/shard_map/all_gather | solution.py:79
  201.0 0.0 copy-start.10
  201.0 6.5 %fusion = f32[512,2048]{1,0:T(8,128)S(1)} fusion(bf16[2,2048,1408]{2,1,0:T(8,128)(2,1)} %all-gather.3.cloned.1.call-done, f32[512,1408]{1,0:T(8,128)} %copy-done, f32[1408]{0:T(1024)S(1)} %copy-done.7), kind=kOutput, calls=%fused_computation.2 | convolution fusion | flops 2954231808 | bytes 12850688 | tf_op jit(solution)/shard_map/dot_general | solution.py:83
  207.5 0.3 copy-done.10
  207.8 4.7 %add_convert_fusion = bf16[512,2048]{1,0:T(8,128)(2,1)} fusion(f32[512,2048]{1,0:T(8,128)S(1)} %fusion, bf16[2,2048,1408]{2,1,0:T(8,128)(2,1)S(1)} %copy-done.10, f32[512,1408]{1,0:T(8,128)S(1)} %get-tuple-element.33, f32[1408]{0:T(1024)S(1)} %copy-done.6), kind=kOutput, calls=%fused_computation.5 | convolution fusion | flops 2956328960 | bytes 14950400 | tf_op jit(solution)/shard_map/dot_general | solution.py:80
  212.5 0.0 reduce-scatter.3.cloned.1.call-update
  212.7 38.3 %all-reduce.8 = (f32[1408]{0:T(1024)}, f32[1408]{0:T(1024)}, f32[3,1408]{1,0:T(4,128)}, f32[3,1408]{1,0:T(4,128)}) all-reduce(f32[1408]{0:T(1024)S(1)} %get-tuple-element.20, f32[1408]{0:T(1024)S(1)} %get-tuple-element.21, f32[3,1408]{1,0:T(4,128)S(1)} %pad_maximum_fusion.1, ...), channel_id=1, replica_groups=mesh['fs'=8,'tp'=4] {'fs'}, use_global_device_ids=true, to_apply=%region_3.4 | all-reduce | flops 11264 | bytes 90112 | tf_op jit(solution)/shard_map/psum | solution.py:71
  251.0 146.0 %reduce-scatter.5.cloned.1.call-done = bf16[256,2816]{0,1:T(8,128)(2,1)} async-done(((bf16[2048,2816]{0,1:T(8,128)(2,1)}), bf16[256,2816]{0,1:T(8,128)(2,1)}) %reduce-scatter.5.cloned.1.call-update) | async-done | bytes 1441808 | tf_op jit(solution)/shard_map/reduce_scatter | solution.py:90
  397.0 1.6 convert_element_type.67
  398.5 0.4 slice_multiply_fusion
  399.0 1.5 copy.17
  400.5 1.5 copy.18
  402.1 28.1 %reduce-scatter.3.cloned.1.call-done = bf16[128,2048]{1,0:T(8,128)(2,1)} async-done(((bf16[512,2048]{1,0:T(8,128)(2,1)}), bf16[128,2048]{1,0:T(8,128)(2,1)}) %reduce-scatter.3.cloned.1.call-update) | async-done | bytes 524304 | tf_op jit(solution)/shard_map/reduce_scatter | solution.py:86
  (8 shorter events, 0.1 us)
Async XLA Ops:
  7.2 27.7 %all-gather.5.cloned.1.call-start = ((), (), s32[]{:S(2)}) async-start(), calls=%async_computation.4 | async-start | bytes 2621440 | tf_op jit(solution)/shard_map/all_gather | solution.py:77
  7.9 193.1 %all-gather.3.cloned.1.call-start = ((), (), s32[]{:S(2)}) async-start(), calls=%async_computation.2 | async-start | bytes 12976128 | tf_op jit(solution)/shard_map/all_gather | solution.py:79
  9.9 1.4 copy-start.8
  9.9 1.4 copy-start.9
  9.9 1.9 copy-start.2
  9.9 2.3 copy-start.4
  9.9 2.3 copy-start.6
  10.0 2.3 copy-start.7
  11.2 385.7 %reduce-scatter.5.cloned.1.call-start = ((), (), s32[]{:S(2)}) async-start(), calls=%async_computation.5 | async-start | bytes 12976128 | tf_op jit(solution)/shard_map/reduce_scatter | solution.py:90
  12.3 1.4 copy-start.1
  13.6 2.8 copy-start.3
  20.1 1.4 copy-start.5
  23.8 1.6 copy-start
  46.2 384.0 %reduce-scatter.3.cloned.1.call-start = ((), (), s32[]{:S(2)}) async-start(), calls=%async_computation.3 | async-start | bytes 2621440 | tf_op jit(solution)/shard_map/reduce_scatter | solution.py:86
  201.0 6.8 %copy-start.10 = (bf16[2,2048,1408]{2,1,0:T(8,128)(2,1)S(1)}, bf16[2,2048,1408]{2,1,0:T(8,128)(2,1)}, u32[]{:S(2)}) copy-start(bf16[2,2048,1408]{2,1,0:T(8,128)(2,1)} %all-gather.3.cloned.1.call-done) | copy-start | bytes 34603012
Sparse Core Ops, SparseCore 0:
  9.5 25.2 all-gather.4
  37.6 163.3 all-gather.2
  204.6 192.3 reduce-scatter.4
  399.9 30.2 reduce-scatter.2
where the time goes:
time: 437 us
  waiting for transfers between devices  338 us (77%)
  blocking collectives  38.3 us (9%)
  matrix products  22.5 us (5%)
  other arithmetic  16.4 us (4%)
  between operations  14 us (3%)
  local copies, waits for them, and re-layouts  7.55 us (2%)
    all_gather x1, waiting for transfers between devices, on_device(): piece = lax.all_gather(stacked, 'fs', axis=1, tiled=True)  155 us
    reduce_scatter x1, waiting for transfers between devices, on_device(): lax.psum_scatter(lax.dot_general(gathered, both_cot, (((0,), (0,)), ((),...  146 us
    psum x1, blocking collectives, on_device(): sums = lax.psum((scale_gate, scale_value, taps_gate, taps_value), 'fs')  38.3 us
    reduce_scatter x1, waiting for transfers between devices, on_device(): lax.psum_scatter(terms.astype(jnp.bfloat16), 'tp', scatter_dimension=0, t...  28.1 us
    dot_general x1, matrix products, on_device(): lax.dot_general(gathered, both_cot, (((0,), (0,)), ((), ())), preferred_e...  11.3 us
  transfers between devices with their start and end apart: 4, of which 4 were waited for; matrix products, arithmetic and copies ran while one was open for 10% of the time, Pallas kernels for 0%

commit v1 on v0

--- a/solution.py
+++ b/solution.py
@@ -71,32 +71,77 @@
     sums = lax.psum((scale_gate, scale_value, taps_gate, taps_value), "fs")
     gate_cot = d_gate_lin.astype(jnp.bfloat16)
     value_cot = d_value_lin.astype(jnp.bfloat16)
-    gate_back = (d_gate_lin * gate_scale).astype(jnp.bfloat16)
-    value_back = (d_value_lin * value_scale).astype(jnp.bfloat16)
-    columns = gate_pre.shape[1]
-    gathered = lax.all_gather(inputs, "tp", axis=0, tiled=True)
-    stacked = jnp.stack([w_gate.astype(jnp.bfloat16), w_value.astype(jnp.bfloat16)])
-    piece = lax.all_gather(stacked, "fs", axis=1, tiled=True)
-    term = lax.dot_general(
-        gate_back, piece[0], (((1,), (1,)), ((), ())), preferred_element_type=jnp.float32
+    n_fs = lax.axis_size("fs")
+    n_tp = lax.axis_size("tp")
+    swap = [(i, i ^ 1) for i in range(n_fs)]
+    groups = [list(range(p, n_fs, 2)) for p in range(2)]
+    parity = lax.axis_index("fs") % 2
+    me = lax.axis_index("tp")
+    rows = w_gate.shape[0]
+    half = rows * n_fs // 2
+    own_tokens = inputs.shape[0]
+
+    split = inputs.reshape(own_tokens, n_fs // 2, 2, rows)
+    keep = lax.dynamic_index_in_dim(split, parity, 2, False).reshape(own_tokens, half)
+    give = lax.dynamic_index_in_dim(split, 1 - parity, 2, False).reshape(own_tokens, half)
+    got = lax.ppermute(give, "fs", swap)
+    tokens = lax.all_gather(jnp.stack([keep, got]), "tp", axis=1, tiled=True)
+
+    scaled = jnp.concatenate(
+        [
+            (w_gate * gate_scale).astype(jnp.bfloat16),
+            (w_value * value_scale).astype(jnp.bfloat16),
+        ],
+        axis=1,
     )
-    terms = term + lax.dot_general(
-        value_back, piece[1], (((1,), (1,)), ((), ())), preferred_element_type=jnp.float32
-    )
-    grad_inputs = lax.psum_scatter(
-        terms.astype(jnp.bfloat16), "tp", scatter_dimension=0, tiled=True
-    )
-    both_cot = jnp.concatenate([gate_cot, value_cot], axis=1)
-    summed = lax.psum_scatter(
-        lax.dot_general(
-            gathered, both_cot, (((0,), (0,)), ((), ())), preferred_element_type=jnp.float32
-        ).astype(jnp.bfloat16),
-        "fs",
-        scatter_dimension=0,
-        tiled=True,
-    ).astype(jnp.float32)
-    grad_w_gate = summed[:, :columns] * gate_scale
-    grad_w_value = summed[:, columns:] * value_scale
+    weights = lax.all_gather(scaled, "fs", axis=0, tiled=True, axis_index_groups=groups)
+
+    columns = gate_cot.shape[1]
+    gate_other = lax.ppermute(gate_cot, "fs", swap)
+    value_other = lax.ppermute(value_cot, "fs", swap)
+
+    def outer(left, right):
+        return lax.dot_general(
+            left, right, (((0,), (0,)), ((), ())), preferred_element_type=jnp.float32
+        )
+
+    def weight_grad(own, other, scale):
+        total = outer(tokens[0], own) + outer(tokens[1], other)
+        summed = lax.psum_scatter(
+            total.astype(jnp.bfloat16), "fs", scatter_dimension=0, tiled=True,
+            axis_index_groups=groups,
+        )
+        return summed.astype(jnp.float32) * scale
+
+    grad_w_gate = weight_grad(gate_cot, gate_other, gate_scale)
+    grad_w_value = weight_grad(value_cot, value_other, value_scale)
+
+    def inner(gate_side, value_side):
+        dims = (((1,), (1,)), ((), ()))
+        return (
+            lax.dot_general(
+                gate_side, weights[:, :columns], dims, preferred_element_type=jnp.float32
+            )
+            + lax.dot_general(
+                value_side, weights[:, columns:], dims, preferred_element_type=jnp.float32
+            )
+        ).astype(jnp.bfloat16)
+
+    def reduce_tp(part):
+        blocks = part.reshape(n_tp, own_tokens, half)
+        total = lax.dynamic_index_in_dim(blocks, me, 0, False).astype(jnp.float32)
+        for shift in range(1, n_tp):
+            block = lax.dynamic_index_in_dim(blocks, (me + shift) % n_tp, 0, False)
+            ring = [(i, (i + shift) % n_tp) for i in range(n_tp)]
+            total = total + lax.ppermute(block, "tp", ring).astype(jnp.float32)
+        return total.astype(jnp.bfloat16)
+
+    mine = reduce_tp(inner(gate_cot, value_cot))
+    theirs = reduce_tp(inner(gate_other, value_other))
+    returned = lax.ppermute(theirs, "fs", swap)
+    even = jnp.where(parity == 0, mine, returned).reshape(own_tokens, n_fs // 2, 1, rows)
+    odd = jnp.where(parity == 0, returned, mine).reshape(own_tokens, n_fs // 2, 1, rows)
+    grad_inputs = jnp.concatenate([even, odd], axis=2).reshape(own_tokens, half * 2)
     return (grad_inputs, grad_w_gate, grad_w_value, sums[0], sums[1], sums[2], sums[3])
 
 

time: 437 us -> 362 us (0.83)
  waiting for transfers between devices: 338 us -> 244 us
  starting transfers between devices: 0.34 us -> 13.3 us
  other arithmetic: 16.4 us -> 23.9 us
    reduce_scatter x2, waiting for transfers between devices: 174 us -> 71.4 us  [weight_grad(): lax.psum_scatter(total.astype(jnp.bfloat16), 'fs', scatter_dimension=0, t...]
    ppermute x0 -> x10, waiting for transfers between devices: none -> 53.4 us  [the longest x1 28.6 us: on_device(): value_other = lax.ppermute(value_cot, 'fs', swap)]
    all_gather x2, waiting for transfers between devices: 163 us -> 119 us  [the longest x1 106 us: on_device(): lax.all_gather(scaled, 'fs', axis=0, tiled=True, axis_index_groups=groups)]
    ppermute x0 -> x10, starting transfers between devices: none -> 12.9 us  [the longest x6 5.05 us: reduce_tp(): total = total + lax.ppermute(block, 'tp', ring).astype(jnp.float32)]
    unnamed x24 -> x31, local copies, waits for them, and re-layouts: 7.42 us -> 2.5 us
    mul x1 -> x2, other arithmetic: 0.44 us -> 5.24 us  [weight_grad(): return summed.astype(jnp.float32) * scale]
    dot_general x3 -> x8, matrix products: 22.5 us -> 25.7 us  [the longest x4 13.6 us: outer(): lax.dot_general(left, right, (((0,), (0,)), ((), ())), preferred_element_...]
  transfers between devices with their start and end apart: 4 -> 14, of which waited for: 4 -> 8; matrix products, arithmetic and copies ran while one was open for 10% -> 9% of each run, Pallas kernels for 0% -> 0%
where the time goes in v1:
time: 362 us; the launch traced here: 361 us
  waiting for transfers between devices  244 us (67%)
  blocking collectives  35.5 us (10%)
  matrix products  25.7 us (7%)
  other arithmetic  23.9 us (7%)
  between operations  14.2 us (4%)
  starting transfers between devices  13.3 us (4%)
  local copies, waits for them, and re-layouts  4.45 us (1%)
    all_gather x1, waiting for transfers between devices, on_device(): lax.all_gather(scaled, 'fs', axis=0, tiled=True, axis_index_groups=groups)  106 us
    reduce_scatter x2, waiting for transfers between devices, weight_grad(): lax.psum_scatter(total.astype(jnp.bfloat16), 'fs', scatter_dimension=0, t...  71.4 us
    psum x1, blocking collectives, on_device(): sums = lax.psum((scale_gate, scale_value, taps_gate, taps_value), 'fs')  35.5 us
    ppermute x1, waiting for transfers between devices, on_device(): value_other = lax.ppermute(value_cot, 'fs', swap)  28.6 us
    ppermute x1, waiting for transfers between devices, on_device(): gate_other = lax.ppermute(gate_cot, 'fs', swap)  14.7 us
    dot_general x4, matrix products, outer(): lax.dot_general(left, right, (((0,), (0,)), ((), ())), preferred_element_...  13.6 us
    all_gather x1, waiting for transfers between devices, on_device(): tokens = lax.all_gather(jnp.stack([keep, got]), 'tp', axis=1, tiled=True)  13 us
  transfers between devices with their start and end apart: 14, of which 8 were waited for; matrix products, arithmetic and copies ran while one was open for 9% of the time, Pallas kernels for 0%

profile of v1, /device:TPU:0, one launch (start us, length us, event | category | flops | bytes accessed | tf_op | source)
XLA Modules:
  0.0 361.3 jit_solution(3099998679081331410)
XLA Ops:
  7.2 0.0 all-gather.5.cloned.1.call-start
  7.3 1.3 copy.23
  8.6 3.1 collective-permute-start.9
  11.7 6.3 %collective-permute-done.9 = bf16[128,1024]{0,1:T(8,128)(2,1)S(1)} collective-permute-done((bf16[128,1024]{0,1:T(8,128)(2,1)S(1)}, bf16[128,1024]{0,1:T(8,128)(2,1)S(1)}, u32[]{:S(2)}, u32[]{:S(2)}) %collective-permute-start.9) | collective-permute-done | bytes 262176 | tf_op jit(solution)/shard_map/ppermute | solution.py:87
  18.0 0.8 pad_maximum_fusion.2
  18.8 0.0 all-gather.5.cloned.1.call-update
  18.9 0.0 copy-start.12
  18.9 0.0 copy-start.13
  18.9 0.0 reduce-scatter.3.cloned.1.call-start
  19.0 0.0 copy-start
  19.0 2.3 convert_multiply_fusion.1
  21.3 0.1 slice_reduce_fusion.4
  21.4 0.0 copy-start.1
  21.4 3.9 %fusion.9 = (f32[512,1408]{1,0:T(8,128)S(1)}, f32[512,1408]{1,0:T(8,128)}) fusion(bf16[512,1408]{1,0:T(8,128)(2,1)S(1)} %copy-done, f32[512,1408]{1,0:T(8,128)S(1)} %get-tuple-element.44, f32[1408]{0:T(1024)S(1)} %get-tuple-element.16, f32[1408]{0:T(1024)S(1)} %get-tuple-element.17, f32[1408]{0:T(1024)S(1)} %get-tuple-element.15, ...), kind=kLoop, calls=%fused_computation.25 | loop fusion | flops 14417920 | bytes 13009920 | tf_op jit(solution)/shard_map/mul | solution.py:43
  25.3 3.2 multiply_reduce_fusion.5
  28.5 1.7 collective-permute-start.3
  30.3 13.0 %all-gather.5.cloned.1.call-done = bf16[2,512,1024]{1,2,0:T(8,128)(2,1)} async-done(((bf16[2,128,1024]{1,2,0:T(8,128)(2,1)}), bf16[2,512,1024]{1,2,0:T(8,128)(2,1)}) %all-gather.5.cloned.1.call-update) | async-done | bytes 2097168 | tf_op jit(solution)/shard_map/all_gather | solution.py:88
  43.3 3.6 fusion.26
  46.9 14.7 %collective-permute-done.3 = bf16[512,1408]{1,0:T(8,128)(2,1)} collective-permute-done((bf16[512,1408]{1,0:T(8,128)(2,1)}, bf16[512,1408]{1,0:T(8,128)(2,1)}, u32[]{:S(2)}, u32[]{:S(2)}) %collective-permute-start.3) | collective-permute-done | bytes 1441824 | tf_op jit(solution)/shard_map/ppermute | solution.py:100
  61.6 4.7 %add_convert_fusion.1 = bf16[1024,1408]{1,0:T(8,128)(2,1)} fusion(f32[1024,1408]{1,0:T(8,128)S(1)} %fusion.26, bf16[512,1408]{1,0:T(8,128)(2,1)} %collective-permute-done.3, bf16[2,512,1024]{1,2,0:T(8,128)(2,1)S(1)} %copy-done.3), kind=kOutput, calls=%fused_computation.1 | convolution fusion | flops 1479278592 | bytes 11141120 | tf_op jit(solution)/shard_map/dot_general | solution.py:104
  66.3 0.0 reduce-scatter.3.cloned.1.call-update
  66.4 0.0 reduce-scatter.5.cloned.1.call-start
  66.4 0.0 copy-start.2
  66.4 3.1 fusion.10
  69.5 2.3 multiply_reduce_fusion.2
  71.9 1.5 collective-permute-start.4
  73.4 1.8 fusion.25
  75.2 28.6 %collective-permute-done.4 = bf16[512,1408]{1,0:T(8,128)(2,1)S(1)} collective-permute-done((bf16[512,1408]{1,0:T(8,128)(2,1)S(1)}, bf16[512,1408]{1,0:T(8,128)(2,1)S(1)}, u32[]{:S(2)}, u32[]{:S(2)}) %collective-permute-start.4) | collective-permute-done | bytes 1441824 | tf_op jit(solution)/shard_map/ppermute | solution.py:101
  103.9 1.1 copy-done.8
  105.0 3.5 add_convert_fusion
  108.4 0.0 reduce-scatter.5.cloned.1.call-update
  108.5 0.2 all-gather.3.cloned.1.call-start
  108.7 15.4 %reduce-scatter.3.cloned.1.call-done = bf16[256,1408]{1,0:T(8,128)(2,1)} async-done(((bf16[1024,1408]{1,0:T(8,128)(2,1)}), bf16[256,1408]{1,0:T(8,128)(2,1)}) %reduce-scatter.3.cloned.1.call-update) | async-done | bytes 720912 | tf_op jit(solution)/shard_map/reduce_scatter | solution.py:110
  124.1 2.4 convert_multiply_fusion.7
  126.4 56.0 %reduce-scatter.5.cloned.1.call-done = bf16[256,1408]{1,0:T(8,128)(2,1)} async-done(((bf16[1024,1408]{1,0:T(8,128)(2,1)}), bf16[256,1408]{1,0:T(8,128)(2,1)}) %reduce-scatter.5.cloned.1.call-update) | async-done | bytes 720912 | tf_op jit(solution)/shard_map/reduce_scatter | solution.py:110
  182.5 2.9 convert_multiply_fusion.6
  185.3 1.3 pad_maximum_fusion
  186.6 0.0 all-gather.3.cloned.1.call-update
  186.7 106.5 %all-gather.3.cloned.1.call-done = bf16[1024,2816]{1,0:T(8,128)(2,1)} async-done(((bf16[256,2816]{1,0:T(8,128)(2,1)}), bf16[1024,2816]{1,0:T(8,128)(2,1)}) %all-gather.3.cloned.1.call-update) | async-done | bytes 5767184 | tf_op jit(solution)/shard_map/all_gather | solution.py:97
  293.2 3.8 %fusion.13 = f32[512,1024]{1,0:T(8,128)S(1)} fusion(bf16[512,1408]{1,0:T(8,128)(2,1)S(1)} %copy-done.9, bf16[1024,2816]{1,0:T(8,128)(2,1)} %all-gather.3.cloned.1.call-done), kind=kOutput, calls=%fused_computation.37 | convolution fusion | flops 1476395008 | bytes 6422528 | tf_op jit(solution)/shard_map/dot_general | solution.py:125
  297.0 3.3 add_convert_fusion.2
  300.3 0.1 dynamic-slice_bitcast_fusion.2
  300.4 0.1 collective-permute-start.5
  300.5 1.5 collective-permute-start.6
  302.0 1.4 collective-permute-start.7
  303.4 1.8 fusion.15
  305.2 3.2 add_convert_fusion.3
  308.4 0.1 dynamic-slice_bitcast_fusion.5
  308.5 0.1 collective-permute-start
  308.5 0.6 collective-permute-start.1
  309.2 0.0 collective-permute-done.5
  309.2 1.4 collective-permute-start.2
  310.6 3.7 %collective-permute-done.7 = bf16[128,1024]{1,0:T(8,128)(2,1)S(1)} collective-permute-done((bf16[128,1024]{1,0:T(8,128)(2,1)S(1)}, bf16[128,1024]{1,0:T(8,128)(2,1)S(1)}, u32[]{:S(2)}, u32[]{:S(2)}) %collective-permute-start.7) | collective-permute-done | bytes 262176 | tf_op jit(solution)/shard_map/ppermute | solution.py:136
  314.3 0.2 fusion.29
  314.5 1.5 collective-permute-start.8
  316.1 35.5 %all-reduce.8 = (f32[1408]{0:T(1024)}, f32[1408]{0:T(1024)}, f32[3,1408]{1,0:T(4,128)}, f32[3,1408]{1,0:T(4,128)}) all-reduce(f32[1408]{0:T(1024)S(1)} %get-tuple-element.13, f32[1408]{0:T(1024)S(1)} %get-tuple-element.14, f32[3,1408]{1,0:T(4,128)S(1)} %pad_maximum_fusion.3, ...), channel_id=1, replica_groups=mesh['fs'=8,'tp'=4] {'fs'}, use_global_device_ids=true, to_apply=%region_3.4 | all-reduce | flops 11264 | bytes 90112 | tf_op jit(solution)/shard_map/psum | solution.py:71
  351.6 0.0 collective-permute-done
  351.6 0.0 collective-permute-done.1
  351.6 0.0 collective-permute-done.8
  351.6 0.2 broadcast_select_fusion.1
  351.9 0.2 reshape.53
  352.2 0.2 reshape.52
  352.4 1.2 pad_maximum_fusion.1
  353.6 1.2 reshape.47
  (36 shorter events, 0.2 us)
Async XLA Ops:
  7.2 11.8 %copy-start.10 = (f32[1408]{0:T(1024)S(1)}, f32[1408]{0:T(1024)}, u32[]{:S(2)}) copy-start(f32[1408]{0:T(1024)} %param.13) | copy-start | bytes 16900
  7.2 11.8 %copy-start.11 = (f32[1408]{0:T(1024)S(1)}, f32[1408]{0:T(1024)}, u32[]{:S(2)}) copy-start(f32[1408]{0:T(1024)} %param.14) | copy-start | bytes 16900
  7.2 36.1 %all-gather.5.cloned.1.call-start = ((), (), s32[]{:S(2)}) async-start(), calls=%async_computation.3 | async-start | bytes 2621440 | tf_op jit(solution)/shard_map/all_gather | solution.py:88
  8.6 9.4 %collective-permute-start.9 = (bf16[128,1024]{0,1:T(8,128)(2,1)S(1)}, bf16[128,1024]{0,1:T(8,128)(2,1)S(1)}, u32[]{:S(2)}, u32[]{:S(2)}) collective-permute-start(bf16[128,1024]{0,1:T(8,128)(2,1)S(1)} %bitcast.47), channel_id=1, source_target_pairs={{0,4},{4,0},{8,12},{12,8},{16,20},{20,16},{24,28},{28,24},{1,5},{5... | collective-permute-start | bytes 786440 | tf_op jit(solution)/shard_map/ppermute | solution.py:87
  18.9 2.4 copy-start.12
  18.9 2.4 copy-start.13
  18.9 105.2 %reduce-scatter.3.cloned.1.call-start = ((), (), s32[]{:S(2)}) async-start(), calls=%async_computation.4 | async-start | bytes 3604480 | tf_op jit(solution)/shard_map/reduce_scatter | solution.py:110
  19.0 2.4 copy-start
  21.4 4.0 %copy-start.1 = (bf16[512,1408]{1,0:T(8,128)(2,1)S(1)}, bf16[512,1408]{1,0:T(8,128)(2,1)}, u32[]{:S(2)}) copy-start(bf16[512,1408]{1,0:T(8,128)(2,1)} %param.17) | copy-start | bytes 4325380
  28.5 33.1 %collective-permute-start.3 = (bf16[512,1408]{1,0:T(8,128)(2,1)}, bf16[512,1408]{1,0:T(8,128)(2,1)}, u32[]{:S(2)}, u32[]{:S(2)}) collective-permute-start(bf16[512,1408]{1,0:T(8,128)(2,1)} %get-tuple-element.26), channel_id=1, source_target_pairs={{0,4},{4,0},{8,12},{12,8},{16,20},{20,16},{24,28},{28,24},{1,5},{5... | collective-permute-start | bytes 4325384 | tf_op jit(solution)/shard_map/ppermute | solution.py:100
  43.3 18.3 %copy-start.3 = (bf16[2,512,1024]{1,2,0:T(8,128)(2,1)S(1)}, bf16[2,512,1024]{1,2,0:T(8,128)(2,1)}, u32[]{:S(2)}) copy-start(bf16[2,512,1024]{1,2,0:T(8,128)(2,1)} %all-gather.5.cloned.1.call-done) | copy-start | bytes 6291460
  66.4 116.1 %reduce-scatter.5.cloned.1.call-start = ((), (), s32[]{:S(2)}) async-start(), calls=%async_computation.5 | async-start | bytes 3604480 | tf_op jit(solution)/shard_map/reduce_scatter | solution.py:110
  66.4 3.1 copy-start.2
  69.5 3.9 %copy-start.4 = (bf16[2,512,1024]{1,2,0:T(8,128)(2,1)S(1)}, bf16[2,512,1024]{1,2,0:T(8,128)(2,1)}, u32[]{:S(2)}) copy-start(bf16[2,512,1024]{1,2,0:T(8,128)(2,1)} %all-gather.5.cloned.1.call-done) | copy-start | bytes 6291460
  71.9 3.3 copy-start.6
  71.9 32.0 %collective-permute-start.4 = (bf16[512,1408]{1,0:T(8,128)(2,1)S(1)}, bf16[512,1408]{1,0:T(8,128)(2,1)S(1)}, u32[]{:S(2)}, u32[]{:S(2)}) collective-permute-start(bf16[512,1408]{1,0:T(8,128)(2,1)S(1)} %get-tuple-element.25), channel_id=1, source_target_pairs={{0,4},{4,0},{8,12},{12,8},{16,20},{20,16},{24,28},{28,24},{1,5},{5... | collective-permute-start | bytes 4325384 | tf_op jit(solution)/shard_map/ppermute | solution.py:101
  103.9 1.1 copy-start.8
  108.4 15.6 %copy-start.5 = (f32[256,1408]{1,0:T(8,128)S(1)}, f32[256,1408]{1,0:T(8,128)}, u32[]{:S(2)}) copy-start(f32[256,1408]{1,0:T(8,128)} %param.11) | copy-start | bytes 4325380
  108.5 184.7 %all-gather.3.cloned.1.call-start = ((), (), s32[]{:S(2)}) async-start(), calls=%async_computation.2 | async-start | bytes 7208960 | tf_op jit(solution)/shard_map/all_gather | solution.py:97
  185.3 107.9 %copy-start.9 = (bf16[512,1408]{1,0:T(8,128)(2,1)S(1)}, bf16[512,1408]{1,0:T(8,128)(2,1)}, u32[]{:S(2)}) copy-start(bf16[512,1408]{1,0:T(8,128)(2,1)} %copy-done.8) | copy-start | bytes 4325380
  293.2 3.8 %copy-start.14 = (bf16[1024,2816]{1,0:T(8,128)(2,1)S(1)}, bf16[1024,2816]{1,0:T(8,128)(2,1)}, u32[]{:S(2)}) copy-start(bf16[1024,2816]{1,0:T(8,128)(2,1)} %all-gather.3.cloned.1.call-done) | copy-start | bytes 17301508
  297.0 6.4 %copy-start.7 = (bf16[512,1408]{1,0:T(8,128)(2,1)S(1)}, bf16[512,1408]{1,0:T(8,128)(2,1)}, u32[]{:S(2)}) copy-start(bf16[512,1408]{1,0:T(8,128)(2,1)} %copy-done.6) | copy-start | bytes 4325380
  300.4 8.8 %collective-permute-start.5 = (bf16[128,1024]{1,0:T(8,128)(2,1)S(1)}, bf16[128,1024]{1,0:T(8,128)(2,1)S(1)}, u32[]{:S(2)}, u32[]{:S(2)}) collective-permute-start(bf16[128,1024]{1,0:T(8,128)(2,1)S(1)} %get-tuple-element.34), channel_id=1, source_target_pairs={{0,1},{1,2},{2,3},{3,0},{4,5},{5,6},{6,7},{7,4},{8,9},{9,10},{10,1... | collective-permute-start | bytes 786440 | tf_op jit(solution)/shard_map/ppermute | solution.py:136
  300.5 10.1 %collective-permute-start.6 = (bf16[128,1024]{1,0:T(8,128)(2,1)S(1)}, bf16[128,1024]{1,0:T(8,128)(2,1)S(1)}, u32[]{:S(2)}, u32[]{:S(2)}) collective-permute-start(bf16[128,1024]{1,0:T(8,128)(2,1)S(1)} %get-tuple-element.36), channel_id=1, source_target_pairs={{0,2},{1,3},{2,0},{3,1},{4,6},{5,7},{6,4},{7,5},{8,10},{9,11},{10,... | collective-permute-start | bytes 786440 | tf_op jit(solution)/shard_map/ppermute | solution.py:136
  302.0 12.3 %collective-permute-start.7 = (bf16[128,1024]{1,0:T(8,128)(2,1)S(1)}, bf16[128,1024]{1,0:T(8,128)(2,1)S(1)}, u32[]{:S(2)}, u32[]{:S(2)}) collective-permute-start(bf16[128,1024]{1,0:T(8,128)(2,1)S(1)} %get-tuple-element.35), channel_id=1, source_target_pairs={{0,3},{1,0},{2,1},{3,2},{4,7},{5,4},{6,5},{7,6},{8,11},{9,8},{10,9... | collective-permute-start | bytes 786440 | tf_op jit(solution)/shard_map/ppermute | solution.py:136
  308.5 43.1 %collective-permute-start = (bf16[128,1024]{1,0:T(8,128)(2,1)S(1)}, bf16[128,1024]{1,0:T(8,128)(2,1)S(1)}, u32[]{:S(2)}, u32[]{:S(2)}) collective-permute-start(bf16[128,1024]{1,0:T(8,128)(2,1)S(1)} %get-tuple-element.31), channel_id=1, source_target_pairs={{0,1},{1,2},{2,3},{3,0},{4,5},{5,6},{6,7},{7,4},{8,9},{9,10},{10,1... | collective-permute-start | bytes 786440 | tf_op jit(solution)/shard_map/ppermute | solution.py:136
  308.5 43.1 %collective-permute-start.1 = (bf16[128,1024]{1,0:T(8,128)(2,1)S(1)}, bf16[128,1024]{1,0:T(8,128)(2,1)S(1)}, u32[]{:S(2)}, u32[]{:S(2)}) collective-permute-start(bf16[128,1024]{1,0:T(8,128)(2,1)S(1)} %get-tuple-element.33), channel_id=1, source_target_pairs={{0,2},{1,3},{2,0},{3,1},{4,6},{5,7},{6,4},{7,5},{8,10},{9,11},{10,... | collective-permute-start | bytes 786440 | tf_op jit(solution)/shard_map/ppermute | solution.py:136
  309.2 42.5 %collective-permute-start.2 = (bf16[128,1024]{1,0:T(8,128)(2,1)S(1)}, bf16[128,1024]{1,0:T(8,128)(2,1)S(1)}, u32[]{:S(2)}, u32[]{:S(2)}) collective-permute-start(bf16[128,1024]{1,0:T(8,128)(2,1)S(1)} %get-tuple-element.32), channel_id=1, source_target_pairs={{0,3},{1,0},{2,1},{3,2},{4,7},{5,4},{6,5},{7,6},{8,11},{9,8},{10,9... | collective-permute-start | bytes 786440 | tf_op jit(solution)/shard_map/ppermute | solution.py:136
  314.5 37.2 %collective-permute-start.8 = (bf16[128,1024]{1,0:T(8,128)(2,1)S(1)}, bf16[128,1024]{1,0:T(8,128)(2,1)S(1)}, u32[]{:S(2)}, u32[]{:S(2)}) collective-permute-start(bf16[128,1024]{1,0:T(8,128)(2,1)S(1)} %fusion.29), channel_id=1, source_target_pairs={{0,4},{4,0},{8,12},{12,8},{16,20},{20,16},{24,28},{28,24},{1,5},{5... | collective-permute-start | bytes 786440 | tf_op jit(solution)/shard_map/ppermute | solution.py:141
Sparse Core Ops, SparseCore 0:
  19.0 24.2 all-gather.4
  66.5 57.5 reduce-scatter.2
  126.4 56.0 reduce-scatter.4
  186.7 106.4 all-gather.2

commit v2 on v1

--- a/solution.py
+++ b/solution.py
@@ -68,13 +68,25 @@
     )
     scale_gate = jnp.sum(d_gate_lin * gate_raw, axis=0)
     scale_value = jnp.sum(d_value_lin * value_raw, axis=0)
-    sums = lax.psum((scale_gate, scale_value, taps_gate, taps_value), "fs")
+    sums = jnp.concatenate([scale_gate[None], scale_value[None], taps_gate, taps_value], axis=0)
+    width = lax.axis_size("fs")
+    if width & (width - 1):
+        sums = lax.psum(sums, "fs")
+    else:
+        step = 1
+        while step < width:
+            sums = sums + lax.ppermute(sums, "fs", [(i, i ^ step) for i in range(width)])
+            step *= 2
     gate_cot = d_gate_lin.astype(jnp.bfloat16)
     value_cot = d_value_lin.astype(jnp.bfloat16)
     n_fs = lax.axis_size("fs")
     n_tp = lax.axis_size("tp")
     swap = [(i, i ^ 1) for i in range(n_fs)]
     groups = [list(range(p, n_fs, 2)) for p in range(2)]
+    ring_size = n_fs // 2
+    place = lax.axis_index("fs") // 2
+    up = [(i, (i + 2) % n_fs) for i in range(n_fs)]
+    down = [(i, (i - 2) % n_fs) for i in range(n_fs)]
     parity = lax.axis_index("fs") % 2
     me = lax.axis_index("tp")
     rows = w_gate.shape[0]
@@ -94,27 +106,68 @@
         ],
         axis=1,
     )
-    weights = lax.all_gather(scaled, "fs", axis=0, tiled=True, axis_index_groups=groups)
-
     columns = gate_cot.shape[1]
     gate_other = lax.ppermute(gate_cot, "fs", swap)
     value_other = lax.ppermute(value_cot, "fs", swap)
+    pieces = [scaled] + [None] * (ring_size - 1)
+    rising = falling = scaled
+    for hop in range(1, ring_size // 2 + 1):
+        if 2 * hop == ring_size:
+            pieces[hop] = jnp.concatenate(
+                [
+                    lax.ppermute(rising[:, :columns], "fs", up),
+                    lax.ppermute(falling[:, columns:], "fs", down),
+                ],
+                axis=1,
+            )
+        else:
+            rising = lax.ppermute(rising, "fs", up)
+            falling = lax.ppermute(falling, "fs", down)
+            if hop == 1:
+                gate_other, rising, falling = lax.optimization_barrier(
+                    (gate_other, rising, falling)
+                )
+            pieces[hop] = rising
+            pieces[ring_size - hop] = falling
+    value_other, pieces = lax.optimization_barrier((value_other, pieces))
+    weights = jnp.concatenate(pieces, axis=0)
+
 
     def outer(left, right):
         return lax.dot_general(
             left, right, (((0,), (0,)), ((), ())), preferred_element_type=jnp.float32
         )
 
-    def weight_grad(own, other, scale):
-        total = outer(tokens[0], own) + outer(tokens[1], other)
-        summed = lax.psum_scatter(
-            total.astype(jnp.bfloat16), "fs", scatter_dimension=0, tiled=True,
-            axis_index_groups=groups,
-        )
-        return summed.astype(jnp.float32) * scale
-
-    grad_w_gate = weight_grad(gate_cot, gate_other, gate_scale)
-    grad_w_value = weight_grad(value_cot, value_other, value_scale)
+    def weight_grad(own, other):
+        return (outer(tokens[0], own) + outer(tokens[1], other)).astype(jnp.bfloat16)
+
+    def ring_scatter(blocks, route, sign):
+        def block(at):
+            return lax.dynamic_index_in_dim(blocks, at % ring_size, 0, False)
+
+        total = block(place - sign + ring_size)
+        for hop in range(1, ring_size):
+            moved = lax.ppermute(total.astype(jnp.bfloat16), "fs", route)
+            total = moved.astype(jnp.float32) + block(
+                place - sign * (1 + hop) + 2 * ring_size
+            ).astype(jnp.float32)
+        return total.astype(jnp.float32)
+
+    gate_total = weight_grad(gate_cot, gate_other)
+    value_total = weight_grad(value_cot, value_other).reshape(ring_size, rows, columns)
+    gate_sum = lax.psum_scatter(
+        gate_total, "fs", scatter_dimension=0, tiled=True, axis_index_groups=groups
+    )
+    middle = (columns // 256) * 128
+    value_sum = jnp.concatenate(
+        [
+            ring_scatter(value_total[:, :, :middle], up, 1),
+            ring_scatter(value_total[:, :, middle:], down, -1),
+        ],
+        axis=1,
+    )
+    grad_w_gate = gate_sum.astype(jnp.float32) * gate_scale
+    grad_w_value = value_sum * value_scale
 
     def inner(gate_side, value_side):
         dims = (((1,), (1,)), ((), ()))
@@ -139,10 +192,15 @@
     mine = reduce_tp(inner(gate_cot, value_cot))
     theirs = reduce_tp(inner(gate_other, value_other))
     returned = lax.ppermute(theirs, "fs", swap)
-    even = jnp.where(parity == 0, mine, returned).reshape(own_tokens, n_fs // 2, 1, rows)
-    odd = jnp.where(parity == 0, returned, mine).reshape(own_tokens, n_fs // 2, 1, rows)
-    grad_inputs = jnp.concatenate([even, odd], axis=2).reshape(own_tokens, half * 2)
-    return (grad_inputs, grad_w_gate, grad_w_value, sums[0], sums[1], sums[2], sums[3])
+    even = jnp.where(parity == 0, mine, returned).reshape(own_tokens, ring_size, rows)
+    odd = jnp.where(parity == 0, returned, mine).reshape(own_tokens, ring_size, rows)
+    parts = []
+    for at in range(ring_size):
+        index = (place - at + ring_size) % ring_size
+        parts.append(lax.dynamic_index_in_dim(even, index, 1, False))
+        parts.append(lax.dynamic_index_in_dim(odd, index, 1, False))
+    grad_inputs = jnp.concatenate(parts, axis=1)
+    return (grad_inputs, grad_w_gate, grad_w_value, sums[0], sums[1], sums[2:5], sums[5:])
 
 
 def solution(mesh):

time: 362 us -> 276 us (0.76)
  waiting for transfers between devices: 244 us -> 143 us
  starting transfers between devices: 13.3 us -> 54.3 us
  blocking collectives: 35.5 us -> 0 us
  local copies, waits for them, and re-layouts: 4.45 us -> 13.1 us
    ppermute x0 -> x13, waiting for transfers between devices: none -> 135 us  [the longest x6 58.7 us: ring_scatter(): moved = lax.ppermute(total.astype(jnp.bfloat16), 'fs', route)]
    all_gather x1 -> x0, waiting for transfers between devices: 106 us -> none  [on_device(): lax.all_gather(scaled, 'fs', axis=0, tiled=True, axis_index_groups=groups)]
    reduce_scatter x2 -> x1, waiting for transfers between devices: 71.4 us -> 0.01 us  [on_device(): lax.psum_scatter(gate_total, 'fs', scatter_dimension=0, tiled=True, axis_...]
    ppermute x0 -> x13, starting transfers between devices: none -> 43.9 us  [the longest x6 31.6 us: ring_scatter(): moved = lax.ppermute(total.astype(jnp.bfloat16), 'fs', route)]
    psum x1 -> x0, blocking collectives: 35.5 us -> none  [on_device(): sums = lax.psum((scale_gate, scale_value, taps_gate, taps_value), 'fs')]
    ppermute x1, waiting for transfers between devices: 28.6 us -> 0.01 us  [on_device(): value_other = lax.ppermute(value_cot, 'fs', swap)]
    ppermute x1, waiting for transfers between devices: 14.7 us -> 0.01 us  [on_device(): gate_other = lax.ppermute(gate_cot, 'fs', swap)]
    all_gather x1, waiting for transfers between devices: 13 us -> 0.01 us  [on_device(): tokens = lax.all_gather(jnp.stack([keep, got]), 'tp', axis=1, tiled=True)]
  transfers between devices with their start and end apart: 14 -> 25, of which waited for: 8 -> 14; matrix products, arithmetic and copies ran while one was open for 9% -> 17% of each run, Pallas kernels for 0% -> 0%
where the time goes in v2:
time: 276 us
  waiting for transfers between devices  143 us (52%)
  starting transfers between devices  54.3 us (20%)
  matrix products  27.5 us (10%)
  other arithmetic  23.2 us (8%)
  between operations  14.5 us (5%)
  local copies, waits for them, and re-layouts  13.1 us (5%)
    ppermute x6, waiting for transfers between devices, ring_scatter(): moved = lax.ppermute(total.astype(jnp.bfloat16), 'fs', route)  58.7 us
    ppermute x3, waiting for transfers between devices, on_device(): lax.ppermute(sums, 'fs', [(i, i ^ step) for i in range(width)])  58.2 us
    ppermute x6, starting transfers between devices, ring_scatter(): moved = lax.ppermute(total.astype(jnp.bfloat16), 'fs', route)  31.6 us
    ppermute x1, waiting for transfers between devices, on_device(): lax.ppermute(falling[:, columns:], 'fs', down)  18.5 us
    dot_general x4, matrix products, outer(): lax.dot_general(left, right, (((0,), (0,)), ((), ())), preferred_element_...  14.7 us
    ppermute x3, starting transfers between devices, on_device(): lax.ppermute(sums, 'fs', [(i, i ^ step) for i in range(width)])  6.41 us
    dot_general x2, matrix products, inner(): lax.dot_general(value_side, weights[:, columns:], dims, preferred_element...  6.41 us
    dot_general x2, matrix products, inner(): lax.dot_general(gate_side, weights[:, :columns], dims, preferred_element_...  6.4 us
  transfers between devices with their start and end apart: 25, of which 14 were waited for; matrix products, arithmetic and copies ran while one was open for 17% of the time, Pallas kernels for 0%

profile of v2, /device:TPU:0, one launch (start us, length us, event | category | flops | bytes accessed | tf_op | source)
XLA Modules:
  0.0 275.6 jit_solution(10351149444716619750)
XLA Ops:
  7.2 0.9 slice_reduce_fusion.7
  8.1 0.9 slice_reduce_fusion.6
  9.0 2.4 convert_multiply_fusion.1
  11.4 0.3 copy-done.2
  11.7 2.8 %multiply_reduce_fusion.1 = (f32[1408]{0:T(1024)S(1)}, f32[1408]{0:T(1024)S(1)}, f32[1408]{0:T(1024)S(1)}, f32[512,1408]{1,0:T(8,128)S(1)}, f32[512,1408]{1,0:T(8,128)S(1)}) fusion(f32[512,1408]{1,0:T(8,128)S(1)} %get-tuple-element.67, f32[1408]{0:T(1024)S(1)} %copy-done.8, bf16[512,1408]{1,0:T(8,128)(2,1)S(1)} %copy-done, ...), kind=kLoop, calls=%fused_computation.30 | loop fusion | flops 13692800 | bytes 14457344 | tf_op jit(solution)/shard_map/reduce_sum | solution.py:55
  14.5 5.2 %multiply_reduce_fusion.4 = (f32[1408]{0:T(1024)S(1)}, f32[1408]{0:T(1024)S(1)}, f32[1408]{0:T(1024)S(1)}, f32[512,1408]{1,0:T(8,128)S(1)}, f32[1408]{0:T(1024)S(1)}, /*index=5*/bf16[512,1408]{1,0:T(8,128)(2,1)}) fusion(f32[512,1408]{1,0:T(8,128)S(1)} %get-tuple-element.66, f32[1408]{0:T(1024)S(1)} %copy-done.7, bf16[512,1408]{1,0:T(8,128)(2,1)S(1)} %copy-done.1, ...), kind=kLoop, calls=%fused_computation.33 | loop fusion | flops 23063040 | bytes 20230144 | tf_op jit(solution)/shard_map/reduce_sum | solution.py:48
  19.7 2.3 fusion.12
  22.0 3.0 %collective-permute-start.1 = (bf16[512,1408]{1,0:T(8,128)(2,1)}, bf16[512,1408]{1,0:T(8,128)(2,1)}, u32[]{:S(2)}, u32[]{:S(2)}) collective-permute-start(bf16[512,1408]{1,0:T(8,128)(2,1)} %get-tuple-element.43), channel_id=1, source_target_pairs={{0,4},{4,0},{8,12},{12,8},{16,20},{20,16},{24,28},{28,24},{1,5},{5... | collective-permute-start | bytes 4325384 | tf_op jit(solution)/shard_map/ppermute | solution.py:110
  25.0 0.2 multiply_convert_fusion
  25.3 1.6 collective-permute-start.2
  26.9 2.2 collective-permute-start.3
  29.1 0.4 collective-permute-start
  29.7 1.7 collective-permute-start.20
  31.4 57.2 %collective-permute-done.20 = f32[8,1408]{1,0:T(8,128)S(1)} collective-permute-done((f32[8,1408]{1,0:T(8,128)S(1)}, f32[8,1408]{1,0:T(8,128)S(1)}, u32[]{:S(2)}, u32[]{:S(2)}) %collective-permute-start.20) | collective-permute-done | bytes 45088 | tf_op jit(solution)/shard_map/ppermute | solution.py:78
  88.6 1.9 collective-permute-start.21
  90.5 1.3 copy.41
  91.8 1.0 collective-permute-done.21
  92.8 0.8 add.351
  93.6 2.8 %collective-permute-start.22 = (f32[8,1408]{1,0:T(8,128)S(1)}, f32[8,1408]{1,0:T(8,128)S(1)}, u32[]{:S(2)}, u32[]{:S(2)}) collective-permute-start(f32[8,1408]{1,0:T(8,128)S(1)} %add.351), channel_id=1, source_target_pairs={{0,16},{4,20},{8,24},{12,28},{16,0},{20,4},{24,8},{28,12},{1,17},{... | collective-permute-start | bytes 135176 | tf_op jit(solution)/shard_map/ppermute | solution.py:78
  96.5 0.9 slice.107
  97.4 1.3 collective-permute-start.5
  98.7 2.1 slice.106
  100.8 0.7 collective-permute-start.4
  101.5 0.8 constant_dynamic-slice_fusion.1
  102.3 1.5 collective-permute-start.13
  103.9 0.6 fusion.50
  104.5 0.6 slice_reduce_fusion
  105.1 3.8 %collective-permute-done.13 = bf16[128,1024]{0,1:T(8,128)(2,1)S(1)} collective-permute-done((bf16[128,1024]{0,1:T(8,128)(2,1)}, bf16[128,1024]{0,1:T(8,128)(2,1)S(1)}, u32[]{:S(2)}, u32[]{:S(2)}) %collective-permute-start.13) | collective-permute-done | bytes 262176 | tf_op jit(solution)/shard_map/ppermute | solution.py:99
  108.9 1.8 pad_maximum_fusion.2
  110.8 18.5 %collective-permute-done.5 = bf16[256,1408]{1,0:T(8,128)(2,1)} collective-permute-done((bf16[256,1408]{1,0:T(8,128)(2,1)}, bf16[256,1408]{1,0:T(8,128)(2,1)}, u32[]{:S(2)}, u32[]{:S(2)}) %collective-permute-start.5) | collective-permute-done | bytes 720928 | tf_op jit(solution)/shard_map/ppermute | solution.py:119
  129.3 1.4 pad_maximum_fusion.1
  130.9 1.5 constant_dynamic-update-slice_fusion.2
  132.5 3.2 %fusion.13 = f32[512,1024]{1,0:T(8,128)S(1)} fusion(bf16[512,1408]{1,0:T(8,128)(2,1)} %collective-permute-done, bf16[1024,2816]{1,0:T(8,128)(2,1)S(1)} %constant_dynamic-update-slice_fusion), kind=kOutput, calls=%fused_computation.37 | convolution fusion | flops 1476395008 | bytes 6422528 | tf_op jit(solution)/shard_map/dot_general | solution.py:178
  135.8 3.2 %add_convert_fusion.2 = bf16[512,1024]{1,0:T(8,128)(2,1)S(1)} fusion(f32[512,1024]{1,0:T(8,128)S(1)} %fusion.13, bf16[512,1408]{1,0:T(8,128)(2,1)} %collective-permute-done.1, bf16[1024,2816]{1,0:T(8,128)(2,1)S(1)} %constant_dynamic-update-slice_fusion), kind=kOutput, calls=%fused_computation.45 | convolution fusion | flops 1477443584 | bytes 7471104 | tf_op jit(solution)/shard_map/dot_general | solution.py:175
  139.1 1.5 collective-permute-start.10
  140.8 3.2 %fusion.15 = f32[512,1024]{1,0:T(8,128)S(1)} fusion(bf16[512,1408]{1,0:T(8,128)(2,1)} %get-tuple-element.65, bf16[1024,2816]{1,0:T(8,128)(2,1)S(1)} %constant_dynamic-update-slice_fusion), kind=kOutput, calls=%fused_computation.39 | convolution fusion | flops 1476395008 | bytes 6422528 | tf_op jit(solution)/shard_map/dot_general | solution.py:178
  144.0 3.2 %add_convert_fusion.3 = bf16[512,1024]{1,0:T(8,128)(2,1)S(1)} fusion(f32[512,1024]{1,0:T(8,128)S(1)} %fusion.15, bf16[512,1408]{1,0:T(8,128)(2,1)} %get-tuple-element.43, bf16[1024,2816]{1,0:T(8,128)(2,1)S(1)} %constant_dynamic-update-slice_fusion), kind=kOutput, calls=%fused_computation.46 | convolution fusion | flops 1477443584 | bytes 7471104 | tf_op jit(solution)/shard_map/dot_general | solution.py:175
  147.2 0.9 dynamic-slice_bitcast_fusion.7
  148.0 1.6 collective-permute-start.8
  149.6 0.6 collective-permute-start.7
  150.2 3.0 %collective-permute-done.10 = bf16[128,1024]{1,0:T(8,128)(2,1)S(1)} collective-permute-done((bf16[128,1024]{1,0:T(8,128)(2,1)S(1)}, bf16[128,1024]{1,0:T(8,128)(2,1)S(1)}, u32[]{:S(2)}, u32[]{:S(2)}) %collective-permute-start.10) | collective-permute-done | bytes 262176 | tf_op jit(solution)/shard_map/ppermute | solution.py:189
  153.2 0.2 collective-permute-done.9
  153.4 0.9 fusion.33
  154.3 1.5 collective-permute-start.12
  155.8 3.6 %fusion.26 = f32[1024,1408]{1,0:T(8,128)S(1)} fusion(bf16[512,1408]{1,0:T(8,128)(2,1)} %get-tuple-element.43, bf16[2,512,1024]{1,2,0:T(8,128)(2,1)} %all-gather.2.cloned.1.call-done), kind=kOutput, calls=%fused_computation.56 | convolution fusion | flops 1476395008 | bytes 8257536 | tf_op jit(solution)/shard_map/dot_general | solution.py:137
  159.5 4.8 %add_convert_fusion.1 = bf16[1024,1408]{1,0:T(8,128)(2,1)} fusion(f32[1024,1408]{1,0:T(8,128)S(1)} %fusion.26, bf16[512,1408]{1,0:T(8,128)(2,1)} %collective-permute-done.1, bf16[2,512,1024]{1,2,0:T(8,128)(2,1)S(1)} %copy-done.3), kind=kOutput, calls=%fused_computation.1 | convolution fusion | flops 1479278592 | bytes 11141120 | tf_op jit(solution)/shard_map/dot_general | solution.py:137
  164.4 0.2 collective-permute-done.6
  164.7 1.3 broadcast_select_fusion
  166.4 0.6 constant_dynamic-slice_fusion.3
  166.9 0.6 constant_dynamic-slice_fusion.2
  167.6 3.2 %fusion.25 = f32[1024,1408]{1,0:T(8,128)S(1)} fusion(bf16[512,1408]{1,0:T(8,128)(2,1)} %get-tuple-element.65, bf16[2,512,1024]{1,2,0:T(8,128)(2,1)S(1)} %copy-done.3), kind=kOutput, calls=%fused_computation.55 | convolution fusion | flops 1476395008 | bytes 8257536 | tf_op jit(solution)/shard_map/dot_general | solution.py:137
  170.7 3.2 %add_convert_fusion = bf16[1024,1408]{1,0:T(8,128)(2,1)S(1)} fusion(f32[1024,1408]{1,0:T(8,128)S(1)} %fusion.25, bf16[512,1408]{1,0:T(8,128)(2,1)} %collective-permute-done, bf16[2,512,1024]{1,2,0:T(8,128)(2,1)S(1)} %copy-done.3), kind=kOutput, calls=%fused_computation | convolution fusion | flops 1479278592 | bytes 11141120 | tf_op jit(solution)/shard_map/dot_general | solution.py:137
  174.2 1.7 collective-permute-start.14
  175.9 2.2 collective-permute-start.17
  178.2 15.5 %collective-permute-done.14 = bf16[256,640]{1,0:T(8,128)(2,1)S(1)} collective-permute-done((bf16[256,640]{1,0:T(8,128)(2,1)S(1)}, bf16[256,640]{1,0:T(8,128)(2,1)S(1)}, u32[]{:S(2)}, u32[]{:S(2)}) %collective-permute-start.14) | collective-permute-done | bytes 327712 | tf_op jit(solution)/shard_map/ppermute | solution.py:150
  193.8 13.7 %collective-permute-start.15 = (bf16[256,640]{1,0:T(8,128)(2,1)S(1)}, bf16[256,640]{1,0:T(8,128)(2,1)S(1)}, u32[]{:S(2)}, u32[]{:S(2)}) collective-permute-start(bf16[256,640]{1,0:T(8,128)(2,1)S(1)} %fusion.30), channel_id=1, source_target_pairs={{0,8},{4,12},{8,16},{12,20},{16,24},{20,28},{24,0},{28,4},{1,9},{5... | collective-permute-start | bytes 983048 | tf_op jit(solution)/shard_map/ppermute | solution.py:150
  207.5 5.0 %collective-permute-done.17 = bf16[256,768]{1,0:T(8,128)(2,1)S(1)} collective-permute-done((bf16[256,768]{1,0:T(8,128)(2,1)S(1)}, bf16[256,768]{1,0:T(8,128)(2,1)S(1)}, u32[]{:S(2)}, u32[]{:S(2)}) %collective-permute-start.17) | collective-permute-done | bytes 393248 | tf_op jit(solution)/shard_map/ppermute | solution.py:150
  212.7 13.6 %collective-permute-done.15 = bf16[256,640]{1,0:T(8,128)(2,1)S(1)} collective-permute-done((bf16[256,640]{1,0:T(8,128)(2,1)S(1)}, bf16[256,640]{1,0:T(8,128)(2,1)S(1)}, u32[]{:S(2)}, u32[]{:S(2)}) %collective-permute-start.15) | collective-permute-done | bytes 327712 | tf_op jit(solution)/shard_map/ppermute | solution.py:150
  226.4 13.8 %collective-permute-start.16 = (bf16[256,640]{1,0:T(8,128)(2,1)S(1)}, bf16[256,640]{1,0:T(8,128)(2,1)S(1)}, u32[]{:S(2)}, u32[]{:S(2)}) collective-permute-start(bf16[256,640]{1,0:T(8,128)(2,1)S(1)} %fusion.29), channel_id=1, source_target_pairs={{0,8},{4,12},{8,16},{12,20},{16,24},{20,28},{24,0},{28,4},{1,9},{5... | collective-permute-start | bytes 983048 | tf_op jit(solution)/shard_map/ppermute | solution.py:150
  240.2 9.4 %collective-permute-done.18 = bf16[256,768]{1,0:T(8,128)(2,1)S(1)} collective-permute-done((bf16[256,768]{1,0:T(8,128)(2,1)S(1)}, bf16[256,768]{1,0:T(8,128)(2,1)S(1)}, u32[]{:S(2)}, u32[]{:S(2)}) %collective-permute-start.18) | collective-permute-done | bytes 393248 | tf_op jit(solution)/shard_map/ppermute | solution.py:150
  249.8 10.0 %collective-permute-done.16 = bf16[256,640]{1,0:T(8,128)(2,1)S(1)} collective-permute-done((bf16[256,640]{1,0:T(8,128)(2,1)S(1)}, bf16[256,640]{1,0:T(8,128)(2,1)S(1)}, u32[]{:S(2)}, u32[]{:S(2)}) %collective-permute-start.16) | collective-permute-done | bytes 327712 | tf_op jit(solution)/shard_map/ppermute | solution.py:150
  259.8 5.3 %collective-permute-done.19 = bf16[256,768]{1,0:T(8,128)(2,1)S(1)} collective-permute-done((bf16[256,768]{1,0:T(8,128)(2,1)S(1)}, bf16[256,768]{1,0:T(8,128)(2,1)S(1)}, u32[]{:S(2)}, u32[]{:S(2)}) %collective-permute-start.19) | collective-permute-done | bytes 393248 | tf_op jit(solution)/shard_map/ppermute | solution.py:150
  265.2 1.2 maximum_multiply_fusion
  266.4 2.3 convert_multiply_fusion.6
  (77 shorter events, 2.6 us)
Async XLA Ops:
  7.2 148.7 %all-gather.2.cloned.1.call-start = ((), (), s32[]{:S(2)}) async-start(), calls=%async_computation.1 | async-start | bytes 2621440 | tf_op jit(solution)/shard_map/all_gather | solution.py:100
  9.0 2.4 copy-start
  9.0 2.7 copy-start.2
  9.0 2.7 copy-start.8
  11.7 2.8 %copy-start.1 = (bf16[512,1408]{1,0:T(8,128)(2,1)S(1)}, bf16[512,1408]{1,0:T(8,128)(2,1)}, u32[]{:S(2)}) copy-start(bf16[512,1408]{1,0:T(8,128)(2,1)} %param.17) | copy-start | bytes 4325380
  11.7 2.8 %copy-start.7 = (f32[1408]{0:T(1024)S(1)}, f32[1408]{0:T(1024)}, u32[]{:S(2)}) copy-start(f32[1408]{0:T(1024)} %param.13) | copy-start | bytes 16900
  19.7 5.3 %copy-start.4 = (f32[256,1408]{1,0:T(8,128)S(1)}, f32[256,1408]{1,0:T(8,128)}, u32[]{:S(2)}) copy-start(f32[256,1408]{1,0:T(8,128)} %param.12) | copy-start | bytes 4325380
  19.7 5.3 %copy-start.5 = (f32[256,1408]{1,0:T(8,128)S(1)}, f32[256,1408]{1,0:T(8,128)}, u32[]{:S(2)}) copy-start(f32[256,1408]{1,0:T(8,128)} %param.11) | copy-start | bytes 4325380
  22.0 74.5 %collective-permute-start.1 = (bf16[512,1408]{1,0:T(8,128)(2,1)}, bf16[512,1408]{1,0:T(8,128)(2,1)}, u32[]{:S(2)}, u32[]{:S(2)}) collective-permute-start(bf16[512,1408]{1,0:T(8,128)(2,1)} %get-tuple-element.43), channel_id=1, source_target_pairs={{0,4},{4,0},{8,12},{12,8},{16,20},{20,16},{24,28},{28,24},{1,5},{5... | collective-permute-start | bytes 4325384 | tf_op jit(solution)/shard_map/ppermute | solution.py:110
  25.3 71.2 %collective-permute-start.2 = (bf16[256,2816]{1,0:T(8,128)(2,1)S(1)}, bf16[256,2816]{1,0:T(8,128)(2,1)}, u32[]{:S(2)}, u32[]{:S(2)}) collective-permute-start(bf16[256,2816]{1,0:T(8,128)(2,1)S(1)} %pad_maximum_fusion), channel_id=1, source_target_pairs={{0,8},{4,12},{8,16},{12,20},{16,24},{20,28},{24,0},{28,4},{1,9},{5... | collective-permute-start | bytes 4325384 | tf_op jit(solution)/shard_map/ppermute | solution.py:124
  26.9 69.6 %collective-permute-start.3 = (bf16[256,2816]{1,0:T(8,128)(2,1)S(1)}, bf16[256,2816]{1,0:T(8,128)(2,1)S(1)}, u32[]{:S(2)}, u32[]{:S(2)}) collective-permute-start(bf16[256,2816]{1,0:T(8,128)(2,1)S(1)} %pad_maximum_fusion), channel_id=1, source_target_pairs={{0,24},{4,28},{8,0},{12,4},{16,8},{20,12},{24,16},{28,20},{1,25},{... | collective-permute-start | bytes 4325384 | tf_op jit(solution)/shard_map/ppermute | solution.py:125
  29.1 101.6 %collective-permute-start = (bf16[512,1408]{1,0:T(8,128)(2,1)}, bf16[512,1408]{1,0:T(8,128)(2,1)}, u32[]{:S(2)}, u32[]{:S(2)}) collective-permute-start(bf16[512,1408]{1,0:T(8,128)(2,1)} %get-tuple-element.65), channel_id=1, source_target_pairs={{0,4},{4,0},{8,12},{12,8},{16,20},{20,16},{24,28},{28,24},{1,5},{5... | collective-permute-start | bytes 4325384 | tf_op jit(solution)/shard_map/ppermute | solution.py:111
  29.7 58.9 %collective-permute-start.20 = (f32[8,1408]{1,0:T(8,128)S(1)}, f32[8,1408]{1,0:T(8,128)S(1)}, u32[]{:S(2)}, u32[]{:S(2)}) collective-permute-start(f32[8,1408]{1,0:T(8,128)S(1)} %concatenate.23), channel_id=1, source_target_pairs={{0,4},{4,0},{8,12},{12,8},{16,20},{20,16},{24,28},{28,24},{1,5},{5... | collective-permute-start | bytes 135176 | tf_op jit(solution)/shard_map/ppermute | solution.py:78
  88.6 4.2 %collective-permute-start.21 = (f32[8,1408]{1,0:T(8,128)S(1)}, f32[8,1408]{1,0:T(8,128)}, u32[]{:S(2)}, u32[]{:S(2)}) collective-permute-start(f32[8,1408]{1,0:T(8,128)S(1)} %add.350), channel_id=1, source_target_pairs={{0,8},{4,12},{8,0},{12,4},{16,24},{20,28},{24,16},{28,20},{1,9},{5... | collective-permute-start | bytes 135176 | tf_op jit(solution)/shard_map/ppermute | solution.py:78
  93.6 10.2 %collective-permute-start.22 = (f32[8,1408]{1,0:T(8,128)S(1)}, f32[8,1408]{1,0:T(8,128)S(1)}, u32[]{:S(2)}, u32[]{:S(2)}) collective-permute-start(f32[8,1408]{1,0:T(8,128)S(1)} %add.351), channel_id=1, source_target_pairs={{0,16},{4,20},{8,24},{12,28},{16,0},{20,4},{24,8},{28,12},{1,17},{... | collective-permute-start | bytes 135176 | tf_op jit(solution)/shard_map/ppermute | solution.py:78
  97.4 31.9 %collective-permute-start.5 = (bf16[256,1408]{1,0:T(8,128)(2,1)}, bf16[256,1408]{1,0:T(8,128)(2,1)}, u32[]{:S(2)}, u32[]{:S(2)}) collective-permute-start(bf16[256,1408]{1,0:T(8,128)(2,1)} %slice.107), channel_id=1, source_target_pairs={{0,24},{4,28},{8,0},{12,4},{16,8},{20,12},{24,16},{28,20},{1,25},{... | collective-permute-start | bytes 2162696 | tf_op jit(solution)/shard_map/ppermute | solution.py:119
  100.8 28.5 %collective-permute-start.4 = (bf16[256,1408]{1,0:T(8,128)(2,1)}, bf16[256,1408]{1,0:T(8,128)(2,1)}, u32[]{:S(2)}, u32[]{:S(2)}) collective-permute-start(bf16[256,1408]{1,0:T(8,128)(2,1)} %slice.106), channel_id=1, source_target_pairs={{0,8},{4,12},{8,16},{12,20},{16,24},{20,28},{24,0},{28,4},{1,9},{5... | collective-permute-start | bytes 2162696 | tf_op jit(solution)/shard_map/ppermute | solution.py:118
  102.3 6.6 %collective-permute-start.13 = (bf16[128,1024]{0,1:T(8,128)(2,1)}, bf16[128,1024]{0,1:T(8,128)(2,1)S(1)}, u32[]{:S(2)}, u32[]{:S(2)}) collective-permute-start(bf16[128,1024]{0,1:T(8,128)(2,1)} %bitcast.20), channel_id=1, source_target_pairs={{0,4},{4,0},{8,12},{12,8},{16,20},{20,16},{24,28},{28,24},{1,5},{5... | collective-permute-start | bytes 786440 | tf_op jit(solution)/shard_map/ppermute | solution.py:99
  110.7 155.7 %reduce-scatter.2.cloned.1.call-start = ((), (), s32[]{:S(2)}) async-start(), calls=%async_computation.2 | async-start | bytes 3604480 | tf_op jit(solution)/shard_map/reduce_scatter | solution.py:158
  139.1 11.2 %collective-permute-start.11 = (bf16[128,1024]{1,0:T(8,128)(2,1)S(1)}, bf16[128,1024]{1,0:T(8,128)(2,1)S(1)}, u32[]{:S(2)}, u32[]{:S(2)}) collective-permute-start(bf16[128,1024]{1,0:T(8,128)(2,1)S(1)} %get-tuple-element.50), channel_id=1, source_target_pairs={{0,3},{1,0},{2,1},{3,2},{4,7},{5,4},{6,5},{7,6},{8,11},{9,8},{10,9... | collective-permute-start | bytes 786440 | tf_op jit(solution)/shard_map/ppermute | solution.py:189
  139.1 14.1 %collective-permute-start.10 = (bf16[128,1024]{1,0:T(8,128)(2,1)S(1)}, bf16[128,1024]{1,0:T(8,128)(2,1)S(1)}, u32[]{:S(2)}, u32[]{:S(2)}) collective-permute-start(bf16[128,1024]{1,0:T(8,128)(2,1)S(1)} %get-tuple-element.51), channel_id=1, source_target_pairs={{0,2},{1,3},{2,0},{3,1},{4,6},{5,7},{6,4},{7,5},{8,10},{9,11},{10,... | collective-permute-start | bytes 786440 | tf_op jit(solution)/shard_map/ppermute | solution.py:189
  140.6 12.8 %collective-permute-start.9 = (bf16[128,1024]{1,0:T(8,128)(2,1)S(1)}, bf16[128,1024]{1,0:T(8,128)(2,1)S(1)}, u32[]{:S(2)}, u32[]{:S(2)}) collective-permute-start(bf16[128,1024]{1,0:T(8,128)(2,1)S(1)} %get-tuple-element.49), channel_id=1, source_target_pairs={{0,1},{1,2},{2,3},{3,0},{4,5},{5,6},{6,7},{7,4},{8,9},{9,10},{10,1... | collective-permute-start | bytes 786440 | tf_op jit(solution)/shard_map/ppermute | solution.py:189
  147.2 8.7 %copy-start.6 = (bf16[512,1024]{1,0:T(8,128)(2,1)}, bf16[512,1024]{1,0:T(8,128)(2,1)S(1)}, u32[]{:S(2)}) copy-start(bf16[512,1024]{1,0:T(8,128)(2,1)S(1)} %add_convert_fusion.3) | copy-start | bytes 3145732
  148.0 16.2 %collective-permute-start.8 = (bf16[128,1024]{1,0:T(8,128)(2,1)}, bf16[128,1024]{1,0:T(8,128)(2,1)S(1)}, u32[]{:S(2)}, u32[]{:S(2)}) collective-permute-start(bf16[128,1024]{1,0:T(8,128)(2,1)} %get-tuple-element.47), channel_id=1, source_target_pairs={{0,3},{1,0},{2,1},{3,2},{4,7},{5,4},{6,5},{7,6},{8,11},{9,8},{10,9... | collective-permute-start | bytes 786440 | tf_op jit(solution)/shard_map/ppermute | solution.py:189
  149.6 14.8 %collective-permute-start.7 = (bf16[128,1024]{1,0:T(8,128)(2,1)S(1)}, bf16[128,1024]{1,0:T(8,128)(2,1)S(1)}, u32[]{:S(2)}, u32[]{:S(2)}) collective-permute-start(bf16[128,1024]{1,0:T(8,128)(2,1)S(1)} %get-tuple-element.48), channel_id=1, source_target_pairs={{0,2},{1,3},{2,0},{3,1},{4,6},{5,7},{6,4},{7,5},{8,10},{9,11},{10,... | collective-permute-start | bytes 786440 | tf_op jit(solution)/shard_map/ppermute | solution.py:189
  150.2 14.4 %collective-permute-start.6 = (bf16[128,1024]{1,0:T(8,128)(2,1)S(1)}, bf16[128,1024]{1,0:T(8,128)(2,1)}, u32[]{:S(2)}, u32[]{:S(2)}) collective-permute-start(bf16[128,1024]{1,0:T(8,128)(2,1)S(1)} %get-tuple-element.46), channel_id=1, source_target_pairs={{0,1},{1,2},{2,3},{3,0},{4,5},{5,6},{6,7},{7,4},{8,9},{9,10},{10,1... | collective-permute-start | bytes 786440 | tf_op jit(solution)/shard_map/ppermute | solution.py:189
  154.3 10.4 %collective-permute-start.12 = (bf16[128,1024]{1,0:T(8,128)(2,1)}, bf16[128,1024]{1,0:T(8,128)(2,1)S(1)}, u32[]{:S(2)}, u32[]{:S(2)}) collective-permute-start(bf16[128,1024]{1,0:T(8,128)(2,1)} %fusion.33), channel_id=1, source_target_pairs={{0,4},{4,0},{8,12},{12,8},{16,20},{20,16},{24,28},{28,24},{1,5},{5... | collective-permute-start | bytes 786440 | tf_op jit(solution)/shard_map/ppermute | solution.py:194
  155.8 3.6 %copy-start.3 = (bf16[2,512,1024]{1,2,0:T(8,128)(2,1)S(1)}, bf16[2,512,1024]{1,2,0:T(8,128)(2,1)}, u32[]{:S(2)}) copy-start(bf16[2,512,1024]{1,2,0:T(8,128)(2,1)} %all-gather.2.cloned.1.call-done) | copy-start | bytes 6291460
  174.2 19.5 %collective-permute-start.14 = (bf16[256,640]{1,0:T(8,128)(2,1)S(1)}, bf16[256,640]{1,0:T(8,128)(2,1)S(1)}, u32[]{:S(2)}, u32[]{:S(2)}) collective-permute-start(bf16[256,640]{1,0:T(8,128)(2,1)S(1)} %dynamic-slice_bitcast_fusion.1), channel_id=1, source_target_pairs={{0,8},{4,12},{8,16},{12,20},{16,24},{20,28},{24,0},{28,4},{1,9},{5... | collective-permute-start | bytes 983048 | tf_op jit(solution)/shard_map/ppermute | solution.py:150
  175.9 36.5 %collective-permute-start.17 = (bf16[256,768]{1,0:T(8,128)(2,1)S(1)}, bf16[256,768]{1,0:T(8,128)(2,1)S(1)}, u32[]{:S(2)}, u32[]{:S(2)}) collective-permute-start(bf16[256,768]{1,0:T(8,128)(2,1)S(1)} %dynamic-slice_bitcast_fusion), channel_id=1, source_target_pairs={{0,24},{4,28},{8,0},{12,4},{16,8},{20,12},{24,16},{28,20},{1,25},{... | collective-permute-start | bytes 1179656 | tf_op jit(solution)/shard_map/ppermute | solution.py:150
  193.8 32.5 %collective-permute-start.15 = (bf16[256,640]{1,0:T(8,128)(2,1)S(1)}, bf16[256,640]{1,0:T(8,128)(2,1)S(1)}, u32[]{:S(2)}, u32[]{:S(2)}) collective-permute-start(bf16[256,640]{1,0:T(8,128)(2,1)S(1)} %fusion.30), channel_id=1, source_target_pairs={{0,8},{4,12},{8,16},{12,20},{16,24},{20,28},{24,0},{28,4},{1,9},{5... | collective-permute-start | bytes 983048 | tf_op jit(solution)/shard_map/ppermute | solution.py:150
  212.6 37.0 %collective-permute-start.18 = (bf16[256,768]{1,0:T(8,128)(2,1)S(1)}, bf16[256,768]{1,0:T(8,128)(2,1)S(1)}, u32[]{:S(2)}, u32[]{:S(2)}) collective-permute-start(bf16[256,768]{1,0:T(8,128)(2,1)S(1)} %fusion.28), channel_id=1, source_target_pairs={{0,24},{4,28},{8,0},{12,4},{16,8},{20,12},{24,16},{28,20},{1,25},{... | collective-permute-start | bytes 1179656 | tf_op jit(solution)/shard_map/ppermute | solution.py:150
  226.4 33.4 %collective-permute-start.16 = (bf16[256,640]{1,0:T(8,128)(2,1)S(1)}, bf16[256,640]{1,0:T(8,128)(2,1)S(1)}, u32[]{:S(2)}, u32[]{:S(2)}) collective-permute-start(bf16[256,640]{1,0:T(8,128)(2,1)S(1)} %fusion.29), channel_id=1, source_target_pairs={{0,8},{4,12},{8,16},{12,20},{16,24},{20,28},{24,0},{28,4},{1,9},{5... | collective-permute-start | bytes 983048 | tf_op jit(solution)/shard_map/ppermute | solution.py:150
  249.7 15.4 %collective-permute-start.19 = (bf16[256,768]{1,0:T(8,128)(2,1)S(1)}, bf16[256,768]{1,0:T(8,128)(2,1)S(1)}, u32[]{:S(2)}, u32[]{:S(2)}) collective-permute-start(bf16[256,768]{1,0:T(8,128)(2,1)S(1)} %fusion.27), channel_id=1, source_target_pairs={{0,24},{4,28},{8,0},{12,4},{16,8},{20,12},{24,16},{28,20},{1,25},{... | collective-permute-start | bytes 1179656 | tf_op jit(solution)/shard_map/ppermute | solution.py:150
  249.8 16.7 %copy-start.9 = (bf16[128,2048]{1,0:T(8,128)(2,1)}, bf16[128,2048]{1,0:T(8,128)(2,1)S(1)}, u32[]{:S(2)}) copy-start(bf16[128,2048]{1,0:T(8,128)(2,1)S(1)} %fusion.37) | copy-start | bytes 1572868
Sparse Core Ops, SparseCore 0:
  110.8 28.6 all-gather.1
  164.4 93.5 reduce-scatter.1
